TPU v7x, 32 devices: a whole 2x2x4 slice. The times are simulated.
32 devices in a mesh: ep: 8 (over z, core), tp: 4 (over y, x).
Axes of the slice: x: 2, y: 2, z: 4, core: 2. Of those that a mesh axis runs over, the one named last changes fastest.
Arguments:
- tokens: bfloat16 [512, 2048], P('ep', 'tp'), as said below
- mix_gain: float32 [2048], replicated, may hold values from 0.1 to 1.9
- w_in: bfloat16 [2048, 1024], P(None, 'tp'), may hold values from -0.125 to 0.125
- a_real: float32 [64, 64], P('tp'), may hold values from -1 to -0.1
- a_imag: float32 [64, 64], P('tp'), may hold values from -3.140625 to 3.140625
- log_step: float32 [64], P('tp'), may hold values from -3 to 0
- b_coef: float32 [2, 64, 64, 16], P(None, 'tp'), may hold values from -2.5 to 2.5
- output_coefficients: float32 [2, 64, 16, 64], P(None, 'tp'), may hold values from -1.25 to 1.25
- skip: float32 [1024], P('tp'), may hold values from -6 to 6
- w_out: bfloat16 [1024, 2048], P('tp'), may hold values from -0.1875 to 0.1875
- state: float32 [2, 512, 64, 64], P(None, 'ep', 'tp'), may hold values from -6 to 6
- ffn_gain: float32 [2048], replicated, may hold values from 0.1 to 1.9
- w_gate: bfloat16 [16, 2048, 4096], P('ep', None, 'tp'), may hold values from -0.125 to 0.125
- w_up: bfloat16 [16, 2048, 4096], P('ep', None, 'tp'), may hold values from -0.125 to 0.125
- w_down: bfloat16 [16, 4096, 2048], P('ep', 'tp'), may hold values from -0.09375 to 0.09375
- expert_ids: int32 [512, 2], P('ep'), may hold values from 0 to 15, all different within a row; in each aligned block of 64 rows (0 to 63, 64 to 127, ...) at most 16 rows name the same one
- route_weights: float32 [512, 2], P('ep'), may hold values from 0.3 to 1
Outputs:
- out: bfloat16 [512, 2048], P('ep', 'tp')
- new_state: float32 [2, 512, 64, 64], P(None, 'ep', 'tp')
Inputs may be any that keep to these rules, and one draw needn't show every extreme that they name: `expert_ids`: A token's 2 experts differ. Among the 64 rows of one index of ep no expert is named more than 16 times, a bound that some block reaches. `tokens`: feature scales differ along the model width.
All inputs are finite; a program needn't handle non-finite values.
Results may differ from a plain program's by a relative error of at most 0.007.
Values may be sent and summed in bfloat16 or wider, within the bound.
A program may use at most 64 MiB of HBM per device.

v0:
```python
import jax
import jax.numpy as jnp
from jax import lax
from jax.sharding import PartitionSpec as P

epsilon = 1e-06
highest_precision = lax.Precision.HIGHEST


def rms_norm(values, gain):
    scaled = values * lax.rsqrt(jnp.mean(values * values, axis=-1, keepdims=True) + epsilon)
    return scaled * gain


def state_update(drive, a_real, a_imag, log_step, b_coef, output_coefficients, skip, state):
    count = drive.shape[0]
    groups = a_real.shape[0]
    drive_float = drive.astype(jnp.float32)
    grouped = drive_float.reshape(count, groups, -1)
    step_size = jnp.exp(log_step)[:, None]
    magnitude = jnp.exp(step_size * a_real)
    decay_re = magnitude * jnp.cos(step_size * a_imag)
    decay_imaginary = magnitude * jnp.sin(step_size * a_imag)
    denominator = a_real * a_real + a_imag * a_imag
    shifted = decay_re - 1.0
    factor_re = (shifted * a_real + decay_imaginary * a_imag) / denominator
    factor_im = (decay_imaginary * a_real - shifted * a_imag) / denominator
    coef_re = factor_re[..., None] * b_coef[0] - factor_im[..., None] * b_coef[1]
    coefficient_imaginary = factor_re[..., None] * b_coef[1] + factor_im[..., None] * b_coef[0]
    push_re = jnp.einsum("gpc,sgc->sgp", coef_re, grouped, precision=highest_precision)
    push_im = jnp.einsum(
        "gpc,sgc->sgp", coefficient_imaginary, grouped, precision=highest_precision
    )
    state_real = decay_re * state[0] - decay_imaginary * state[1] + push_re
    state_imaginary = decay_re * state[1] + decay_imaginary * state[0] + push_im
    state_readout = jnp.einsum(
        "amz,daz->dam", output_coefficients[0], state_real, precision=highest_precision
    ) - jnp.einsum(
        "amz,daz->dam", output_coefficients[1], state_imaginary, precision=highest_precision
    )
    mixed = state_readout.reshape(count, -1) + skip * drive_float
    return (jax.nn.gelu(mixed).astype(jnp.bfloat16), jnp.stack([state_real, state_imaginary]))


def slot_table(expert_ids, experts, capacity):
    flat_ids = expert_ids.reshape(-1)
    onehot = (flat_ids[:, None] == jnp.arange(experts, dtype=jnp.int32)[None, :]).astype(jnp.int32)
    ranks = jnp.cumsum(onehot, axis=0) - 1
    slot_rank = jnp.sum(onehot * ranks, axis=1)
    slots = flat_ids * capacity + slot_rank
    return (slots[:, None] == jnp.arange(experts * capacity, dtype=jnp.int32)[None, :]).astype(
        jnp.float32
    )


def local(
    tokens,
    mix_gain,
    w_in,
    a_real,
    a_imag,
    log_step,
    b_coef,
    output_coefficients,
    skip,
    w_out,
    state,
    ffn_gain,
    w_gate,
    w_up,
    w_down,
    expert_ids,
    route_weights,
):
    seq_count = tokens.shape[0]
    width = tokens.shape[1]
    top_count = expert_ids.shape[1]
    ep_count = lax.axis_size("ep")
    tp_count = lax.axis_size("tp")
    model_width = width * tp_count
    local_experts = w_gate.shape[0]
    experts = local_experts * ep_count
    capacity = max(2, 2 * seq_count * top_count // experts)
    col_start = lax.axis_index("tp") * width
    whole_rows = lax.all_gather(tokens, "tp", axis=1, tiled=True)
    tok_float = whole_rows.astype(jnp.float32)
    normed = rms_norm(tok_float, mix_gain).astype(jnp.bfloat16)
    drive = jnp.dot(normed, w_in, preferred_element_type=jnp.float32).astype(jnp.bfloat16)
    mixed, new_state = state_update(
        drive, a_real, a_imag, log_step, b_coef, output_coefficients, skip, state
    )
    partial_mix = jnp.dot(mixed, w_out, preferred_element_type=jnp.float32)
    placed = slot_table(expert_ids, experts, capacity)
    per_token = (
        placed.reshape(seq_count, top_count, experts * capacity).sum(axis=1).astype(jnp.bfloat16)
    )
    mix_full = lax.psum(partial_mix, "tp")
    resid_full = (tok_float + mix_full).astype(jnp.bfloat16)
    normed2 = rms_norm(resid_full.astype(jnp.float32), ffn_gain).astype(jnp.bfloat16)
    resid_own = lax.dynamic_slice_in_dim(resid_full, col_start, width, 1)
    send_buffer = jnp.dot(per_token.T, normed2, preferred_element_type=jnp.float32).astype(
        jnp.bfloat16
    )
    send_buffer = send_buffer.reshape(ep_count, local_experts, capacity, model_width)
    slot_rows = lax.all_to_all(send_buffer, "ep", split_axis=0, concat_axis=0, tiled=True)
    gate_vals = jnp.einsum("njcd,jdf->njcf", slot_rows, w_gate, preferred_element_type=jnp.float32)
    up_vals = jnp.einsum("njcd,jdf->njcf", slot_rows, w_up, preferred_element_type=jnp.float32)
    hidden = (jax.nn.silu(gate_vals) * up_vals).astype(jnp.bfloat16)
    partial_out = jnp.einsum("njcf,jfd->njcd", hidden, w_down, preferred_element_type=jnp.float32)
    expert_result = lax.psum_scatter(
        partial_out.astype(jnp.bfloat16), "tp", scatter_dimension=3, tiled=True
    )
    returned_rows = lax.all_to_all(expert_result, "ep", split_axis=0, concat_axis=0, tiled=True)
    returned_rows = returned_rows.reshape(experts * capacity, width).astype(jnp.float32)
    weighted = placed * route_weights.reshape(-1)[:, None]
    combined = jnp.dot(weighted, returned_rows, precision=highest_precision)
    combined = combined.reshape(seq_count, top_count, width).sum(axis=1)
    out = (resid_own.astype(jnp.float32) + combined).astype(jnp.bfloat16)
    return (out, new_state)


def solution(mesh):
    in_specs = (
        P("ep", "tp"),
        P(),
        P(None, "tp"),
        P("tp", None),
        P("tp", None),
        P("tp"),
        P(None, "tp", None, None),
        P(None, "tp", None, None),
        P("tp"),
        P("tp", None),
        P(None, "ep", "tp", None),
        P(),
        P("ep", None, "tp"),
        P("ep", None, "tp"),
        P("ep", "tp", None),
        P("ep", None),
        P("ep", None),
    )
    out_specs = (P("ep", "tp"), P(None, "ep", "tp", None))
    return jax.shard_map(local, mesh=mesh, in_specs=in_specs, out_specs=out_specs, check_vma=False)
```

profile of v0, /device:TPU:0, one launch (start us, length us, event | category | flops | bytes accessed | tf_op | source)
XLA Modules:
  0.0 168.2 jit_solution(7657873128458054456)
XLA Ops:
  7.3 10.9 %all_gather.3 = bf16[64,2048]{1,0:T(8,128)(2,1)S(1)} all-gather(bf16[64,512]{1,0:T(8,128)(2,1)} %param.17), channel_id=1, replica_groups=mesh['ep'=8,'tp'=4] {'tp'}, dimensions={1}, use_global_device_ids=true | all-gather | bytes 327680 | tf_op jit(solution)/shard_map/all_gather | solution.py:85
  18.2 0.2 fusion.31
  18.3 1.6 convolution_convert_fusion.1
  19.9 0.1 copy.68
  20.0 0.7 exp.10
  20.7 1.3 fusion.87
  22.0 0.8 fusion.80
  22.8 1.6 fusion.24
  24.4 1.6 fusion.25
  26.1 1.8 %fusion.43 = f32[16,64,16]{1,2,0:T(8,128)S(1)} fusion(f32[64,16,64]{2,0,1:T(8,128)S(1)} %fusion.25, f32[2,16,16,64]{3,2,1,0:T(8,128)} %param.24), kind=kOutput, calls=%fused_computation.43 | convolution fusion | flops 12582912 | bytes 458752 | tf_op jit(solution)/shard_map/amz,daz->dam/dot_general | solution.py:36
  27.9 0.9 convolution_subtract_fusion
  29.0 1.1 fusion.72
  30.2 0.1 eq.49
  30.5 0.2 reduce_window_sum.11
  30.6 0.2 select_reduce_fusion
  30.8 0.1 reduce_sum.49
  31.2 44.7 %all-reduce.2.cloned.1.call-done = f32[64,2048]{1,0:T(8,128)} async-done(((f32[64,2048]{1,0:T(8,128)}), f32[64,2048]{1,0:T(8,128)}) %all-reduce.2.cloned.1.call-update) | async-done | bytes 524304 | tf_op jit(solution)/shard_map/psum | solution.py:97
  75.9 1.2 fusion.28
  77.1 0.5 convolution_convert_fusion
  77.6 31.2 %all_to_all.10 = bf16[8,2,16,2048]{3,2,1,0:T(8,128)(2,1)S(1)} all-to-all(bf16[8,2,16,2048]{3,2,1,0:T(8,128)(2,1)S(1)} %bitcast.107), channel_id=1, replica_groups=mesh['ep'=8,'tp'=4] {'ep'}, dimensions={0} | all-to-all | bytes 2097152 | tf_op jit(solution)/shard_map/all_to_all | solution.py:105
  108.9 4.8 %fusion.12 = f32[8,2,16,1024]{3,2,0,1:T(8,128)S(1)} fusion(bf16[2,2048,1024]{2,1,0:T(8,128)(2,1)} %param.29, bf16[8,2,16,2048]{3,2,1,0:T(8,128)(2,1)S(1)} %all_to_all.10), kind=kOutput, calls=%fused_computation.9 | convolution fusion | flops 1073741824 | bytes 10485760 | tf_op jit(solution)/shard_map/njcd,jdf->njcf/dot_general | solution.py:106
  113.7 1.4 fusion.21
  115.1 1.0 slice-done.1
  116.1 2.2 %fusion.9 = bf16[8,2,16,2048]{3,2,0,1:T(8,128)(2,1)} fusion(bf16[8,2,16,1024]{3,2,0,1:T(8,128)(2,1)S(1)} %fusion.21, bf16[2,1024,2048]{2,1,0:T(8,128)(2,1)S(1)} %bitcast.104), kind=kOutput, calls=%fused_computation.8 | convolution fusion | flops 1074266112 | bytes 9961472 | tf_op jit(solution)/shard_map/njcf,jfd->njcd/dot_general | solution.py:109
  118.4 26.0 %reduce-scatter.2.cloned.1.call-done = bf16[8,2,16,512]{3,2,0,1:T(8,128)(2,1)} async-done(((bf16[8,2,16,2048]{3,2,0,1:T(8,128)(2,1)}), bf16[8,2,16,512]{3,2,0,1:T(8,128)(2,1)}) %reduce-scatter.2.cloned.1.call-update) | async-done | bytes 262160 | tf_op jit(solution)/shard_map/reduce_scatter | solution.py:110
  144.4 1.7 copy.74
  146.1 4.6 %all-to-all-start.1 = ((bf16[8,2,16,512]{3,2,1,0:T(8,128)(2,1)}), bf16[8,2,16,512]{3,2,1,0:T(8,128)(2,1)S(1)}, u32[]{:S(2)}, u32[]{:S(2)}) async-start(bf16[8,2,16,512]{3,2,1,0:T(8,128)(2,1)} %copy.74), calls=%async_computation.2 | async-start | bytes 524288 | tf_op jit(solution)/shard_map/all_to_all | solution.py:113
  150.7 0.1 pad_maximum_fusion
  150.8 1.6 copy.75
  152.4 8.0 %all-to-all-done.1 = bf16[8,2,16,512]{3,2,1,0:T(8,128)(2,1)S(1)} async-done(((bf16[8,2,16,512]{3,2,1,0:T(8,128)(2,1)}), bf16[8,2,16,512]{3,2,1,0:T(8,128)(2,1)S(1)}, u32[]{:S(2)}, u32[]{:S(2)}) %all-to-all-start.1) | async-done | bytes 262176 | tf_op jit(solution)/shard_map/all_to_all | solution.py:113
  160.4 0.3 convolution_reduce_fusion
  160.8 0.7 add_convert_fusion
  (33 shorter events, 0.6 us)
Async XLA Ops:
  7.2 21.8 %copy-start = (bf16[256,2048]{1,0:T(8,128)(2,1)S(1)}, bf16[256,2048]{1,0:T(8,128)(2,1)}, u32[]{:S(2)}) copy-start(bf16[256,2048]{1,0:T(8,128)(2,1)} %param.26) | copy-start | bytes 3145732
  7.2 20.7 %copy-start.1 = (f32[2,16,16,64]{3,2,1,0:T(8,128)S(1)}, f32[2,16,16,64]{3,2,1,0:T(8,128)}, u32[]{:S(2)}) copy-start(f32[2,16,16,64]{3,2,1,0:T(8,128)} %param.24) | copy-start | bytes 393220
  7.2 21.8 %copy-start.5 = (f32[256]{0:T(256)S(1)}, f32[256]{0:T(256)}, u32[]{:S(2)}) copy-start(f32[256]{0:T(256)} %param.25) | copy-start | bytes 3076
  7.2 22.9 %copy-start.3 = (s32[64,2]{0,1:T(2,128)S(1)}, s32[64,2]{0,1:T(2,128)}, u32[]{:S(2)}) copy-start(s32[64,2]{0,1:T(2,128)} %param.32) | copy-start | bytes 1540
  7.2 69.9 %copy-start.2 = (f32[2048]{0:T(1024)S(1)}, f32[2048]{0:T(1024)}, u32[]{:S(2)}) copy-start(f32[2048]{0:T(1024)} %param.28) | copy-start | bytes 24580
  7.2 68.7 %all-reduce.2.cloned.1.call-start = ((), (), s32[]{:S(2)}) async-start(), calls=%async_computation.3 | async-start | bytes 1048576 | tf_op jit(solution)/shard_map/psum | solution.py:97
  30.1 114.4 %reduce-scatter.2.cloned.1.call-start = ((), (), s32[]{:S(2)}) async-start(), calls=%async_computation.4 | async-start | bytes 1310720 | tf_op jit(solution)/shard_map/reduce_scatter | solution.py:110
  77.6 36.0 %slice-start.2 = ((s8[8388608]{0:T(1024)(128)(4,1)}), s8[4194304]{0:T(1024)(128)(4,1)S(1)}, s32[]{:S(2)}) async-start(s8[8388608]{0:T(1024)(128)(4,1)} %bitcast.112), calls=%async_computation.7 | async-start | bytes 8388608
  108.9 4.8 %slice-start.3 = ((s8[8388608]{0:T(1024)(128)(4,1)}), s8[4194304]{0:T(1024)(128)(4,1)S(1)}, s32[]{:S(2)}) async-start(s8[8388608]{0:T(1024)(128)(4,1)} %bitcast.112), calls=%async_computation.8 | async-start | bytes 8388608
  108.9 6.3 %slice-start = ((s8[8388608]{0:T(1024)(128)(4,1)}), s8[4194304]{0:T(1024)(128)(4,1)S(1)}, s32[]{:S(2)}) async-start(s8[8388608]{0:T(1024)(128)(4,1)} %bitcast.103), calls=%async_computation.5 | async-start | bytes 8388608
  113.7 2.5 %slice-start.1 = ((s8[8388608]{0:T(1024)(128)(4,1)}), s8[4194304]{0:T(1024)(128)(4,1)S(1)}, s32[]{:S(2)}) async-start(s8[8388608]{0:T(1024)(128)(4,1)} %bitcast.103), calls=%async_computation.6 | async-start | bytes 8388608
  116.1 44.3 %copy-start.4 = (f32[64,2]{0,1:T(2,128)S(1)}, f32[64,2]{0,1:T(2,128)}, u32[]{:S(2)}) copy-start(f32[64,2]{0,1:T(2,128)} %param.33) | copy-start | bytes 1540
  146.1 14.3 %all-to-all-start.1 = ((bf16[8,2,16,512]{3,2,1,0:T(8,128)(2,1)}), bf16[8,2,16,512]{3,2,1,0:T(8,128)(2,1)S(1)}, u32[]{:S(2)}, u32[]{:S(2)}) async-start(bf16[8,2,16,512]{3,2,1,0:T(8,128)(2,1)} %copy.74), calls=%async_computation.2 | async-start | bytes 524288 | tf_op jit(solution)/shard_map/all_to_all | solution.py:113
Sparse Core Ops, SparseCore 0:
  30.2 45.6 all-reduce.1
  118.5 25.8 reduce-scatter.1
where the time goes:
time: 169 us; the launch traced here: 168 us
  waiting for transfers between devices  78.8 us (47%)
  blocking collectives  42.1 us (25%)
  matrix products  18 us (11%)
  between operations  14.3 us (8%)
  local copies, waits for them, and re-layouts  6.87 us (4%)
  starting transfers between devices  4.69 us (3%)
  other arithmetic  3.53 us (2%)
    psum x1, waiting for transfers between devices, local(): mix_full = lax.psum(partial_mix, 'tp')  44.7 us
    all_to_all x1, blocking collectives, local(): lax.all_to_all(send_buffer, 'ep', split_axis=0, concat_axis=0, tiled=True)  31.2 us
    reduce_scatter x1, waiting for transfers between devices, local(): lax.psum_scatter(partial_out.astype(jnp.bfloat16), 'tp', scatter_dimensio...  26 us
    all_gather x1, blocking collectives, local(): whole_rows = lax.all_gather(tokens, 'tp', axis=1, tiled=True)  10.9 us
    all_to_all x1, waiting for transfers between devices, local(): lax.all_to_all(expert_result, 'ep', split_axis=0, concat_axis=0, tiled=True)  8.01 us
    dot_general x1, matrix products, local(): jnp.einsum('njcd,jdf->njcf', slot_rows, w_gate, preferred_element_type=jn...  4.78 us
    all_to_all x1, starting transfers between devices, local(): lax.all_to_all(expert_result, 'ep', split_axis=0, concat_axis=0, tiled=True)  4.61 us
  transfers between devices with their start and end apart: 3, of which 3 were waited for; matrix products, arithmetic and copies ran while one was open for 2% of the time, Pallas kernels for 0%

commit v1 on v0

--- a/solution.py
+++ b/solution.py
@@ -94,7 +94,8 @@
     per_token = (
         placed.reshape(seq_count, top_count, experts * capacity).sum(axis=1).astype(jnp.bfloat16)
     )
-    mix_full = lax.psum(partial_mix, "tp")
+    parts = lax.all_gather(partial_mix, "tp")
+    mix_full = jnp.sum(parts, axis=0)
     resid_full = (tok_float + mix_full).astype(jnp.bfloat16)
     normed2 = rms_norm(resid_full.astype(jnp.float32), ffn_gain).astype(jnp.bfloat16)
     resid_own = lax.dynamic_slice_in_dim(resid_full, col_start, width, 1)

time: 169 us -> 159 us (0.941)
  waiting for transfers between devices: 78.8 us -> 68.6 us
    psum x1 -> x0, waiting for transfers between devices: 44.7 us -> none  [local(): mix_full = lax.psum(partial_mix, 'tp')]
    all_gather x0 -> x1, waiting for transfers between devices: none -> 34.5 us  [local(): parts = lax.all_gather(partial_mix, 'tp')]
    reduce_sum x0 -> x1, other arithmetic: none -> 1.76 us  [local(): mix_full = jnp.sum(parts, axis=0)]
where the time goes in v1:
time: 159 us
  waiting for transfers between devices  68.6 us (43%)
  blocking collectives  42.1 us (26%)
  matrix products  17.9 us (11%)
  between operations  14.3 us (9%)
  local copies, waits for them, and re-layouts  6.88 us (4%)
  starting transfers between devices  4.69 us (3%)
  other arithmetic  4.25 us (3%)
    all_gather x1, waiting for transfers between devices, local(): parts = lax.all_gather(partial_mix, 'tp')  34.5 us
    all_to_all x1, blocking collectives, local(): lax.all_to_all(send_buffer, 'ep', split_axis=0, concat_axis=0, tiled=True)  31.2 us
    reduce_scatter x1, waiting for transfers between devices, local(): lax.psum_scatter(partial_out.astype(jnp.bfloat16), 'tp', scatter_dimensio...  26 us
    all_gather x1, blocking collectives, local(): whole_rows = lax.all_gather(tokens, 'tp', axis=1, tiled=True)  10.9 us
    all_to_all x1, waiting for transfers between devices, local(): lax.all_to_all(expert_result, 'ep', split_axis=0, concat_axis=0, tiled=True)  8.01 us
    dot_general x1, matrix products, local(): jnp.einsum('njcd,jdf->njcf', slot_rows, w_gate, preferred_element_type=jn...  4.78 us
    all_to_all x1, starting transfers between devices, local(): lax.all_to_all(expert_result, 'ep', split_axis=0, concat_axis=0, tiled=True)  4.61 us
  transfers between devices with their start and end apart: 3, of which 3 were waited for; matrix products, arithmetic and copies ran while one was open for 2% of the time, Pallas kernels for 0%

profile of v1, /device:TPU:0, one launch (start us, length us, event | category | flops | bytes accessed | tf_op | source)
XLA Modules:
  0.0 158.8 jit_solution(669779991791791203)
XLA Ops:
  7.3 10.9 %all_gather.9 = bf16[64,2048]{1,0:T(8,128)(2,1)S(1)} all-gather(bf16[64,512]{1,0:T(8,128)(2,1)} %param.17), channel_id=1, replica_groups=mesh['ep'=8,'tp'=4] {'tp'}, dimensions={1}, use_global_device_ids=true | all-gather | bytes 327680 | tf_op jit(solution)/shard_map/all_gather | solution.py:85
  18.2 0.2 fusion.31
  18.3 1.6 convolution_convert_fusion.1
  19.9 0.1 copy.68
  20.0 0.7 exp.10
  20.7 1.3 fusion.87
  22.0 0.8 fusion.80
  22.8 1.6 %fusion.24 = f32[64,16,64]{2,0,1:T(8,128)S(1)} fusion(bf16[64,16,16]{0,2,1:T(8,128)(2,1)S(1)} %bitcast.111, f32[1,64,16,64]{3,2,1,0:T(8,128)S(1)} %get-tuple-element.15, f32[1,64,16,64]{3,2,1,0:T(8,128)S(1)} %get-tuple-element.14, f32[16,64]{1,0:T(8,128)S(1)} %get-tuple-element.17, f32[16,64]{1,0:T(8,128)S(1)} %get-tuple-element.18, ...), kind=kOutput, calls=%fused_computation.14 | convolution fusion | flops 12894208 | bytes 966656 | tf_op jit(solution)/shard_map/gpc,sgc->sgp/dot_general | solution.py:31
  24.4 1.6 %fusion.25 = f32[64,16,64]{2,0,1:T(8,128)S(1)} fusion(bf16[64,16,16]{0,2,1:T(8,128)(2,1)S(1)} %bitcast.112, f32[1,64,16,64]{3,2,1,0:T(8,128)S(1)} %get-tuple-element.15, f32[1,64,16,64]{3,2,1,0:T(8,128)S(1)} %get-tuple-element.14, f32[16,64]{1,0:T(8,128)S(1)} %get-tuple-element.17, f32[16,64]{1,0:T(8,128)S(1)} %get-tuple-element.18, ...), kind=kOutput, calls=%fused_computation.16 | convolution fusion | flops 12894208 | bytes 966656 | tf_op jit(solution)/shard_map/gpc,sgc->sgp/dot_general | solution.py:30
  26.1 1.8 %fusion.43 = f32[16,64,16]{1,2,0:T(8,128)S(1)} fusion(f32[64,16,64]{2,0,1:T(8,128)S(1)} %fusion.25, f32[2,16,16,64]{3,2,1,0:T(8,128)} %param.24), kind=kOutput, calls=%fused_computation.43 | convolution fusion | flops 12582912 | bytes 458752 | tf_op jit(solution)/shard_map/amz,daz->dam/dot_general | solution.py:36
  27.9 0.9 convolution_subtract_fusion
  29.0 1.1 fusion.72
  30.2 0.1 eq.49
  30.5 0.2 reduce_window_sum.11
  30.6 0.2 select_reduce_fusion
  30.8 0.1 reduce_sum.59
  31.2 34.5 %all-gather.3.cloned.1.call-done = f32[256,2048]{1,0:T(8,128)} async-done(((f32[64,2048]{1,0:T(8,128)}), f32[256,2048]{1,0:T(8,128)}) %all-gather.3.cloned.1.call-update) | async-done | bytes 2097168 | tf_op jit(solution)/shard_map/all_gather | solution.py:97
  65.7 1.8 %reduce_sum.57 = f32[64,2048]{1,0:T(8,128)S(1)} reduce(f32[4,64,2048]{2,1,0:T(8,128)} %bitcast.109, f32[]{:T(128)} %constant.14.clone.1), dimensions={0}, to_apply=%region_1.0 | reduce | flops 393216 | bytes 2621444 | tf_op jit(solution)/shard_map/reduce_sum | solution.py:98
  67.4 0.2 fusion.28
  67.6 0.5 convolution_convert_fusion
  68.1 31.2 %all_to_all.10 = bf16[8,2,16,2048]{3,2,1,0:T(8,128)(2,1)S(1)} all-to-all(bf16[8,2,16,2048]{3,2,1,0:T(8,128)(2,1)S(1)} %bitcast.108), channel_id=1, replica_groups=mesh['ep'=8,'tp'=4] {'ep'}, dimensions={0} | all-to-all | bytes 2097152 | tf_op jit(solution)/shard_map/all_to_all | solution.py:106
  99.4 4.8 %fusion.12 = f32[8,2,16,1024]{3,2,0,1:T(8,128)S(1)} fusion(bf16[2,2048,1024]{2,1,0:T(8,128)(2,1)} %param.29, bf16[8,2,16,2048]{3,2,1,0:T(8,128)(2,1)S(1)} %all_to_all.10), kind=kOutput, calls=%fused_computation.9 | convolution fusion | flops 1073741824 | bytes 10485760 | tf_op jit(solution)/shard_map/njcd,jdf->njcf/dot_general | solution.py:107
  104.2 1.4 fusion.21
  105.6 1.0 slice-done.1
  106.7 2.2 %fusion.9 = bf16[8,2,16,2048]{3,2,0,1:T(8,128)(2,1)} fusion(bf16[8,2,16,1024]{3,2,0,1:T(8,128)(2,1)S(1)} %fusion.21, bf16[2,1024,2048]{2,1,0:T(8,128)(2,1)S(1)} %bitcast.105), kind=kOutput, calls=%fused_computation.8 | convolution fusion | flops 1074266112 | bytes 9961472 | tf_op jit(solution)/shard_map/njcf,jfd->njcd/dot_general | solution.py:110
  108.9 26.0 %reduce-scatter.2.cloned.1.call-done = bf16[8,2,16,512]{3,2,0,1:T(8,128)(2,1)} async-done(((bf16[8,2,16,2048]{3,2,0,1:T(8,128)(2,1)}), bf16[8,2,16,512]{3,2,0,1:T(8,128)(2,1)}) %reduce-scatter.2.cloned.1.call-update) | async-done | bytes 262160 | tf_op jit(solution)/shard_map/reduce_scatter | solution.py:111
  135.0 1.7 %copy.74 = bf16[8,2,16,512]{3,2,1,0:T(8,128)(2,1)} copy(bf16[8,2,16,512]{3,2,0,1:T(8,128)(2,1)} %reduce-scatter.2.cloned.1.call-done) | data formatting | bytes 524288 | tf_op jit(solution)/shard_map/reduce_scatter | solution.py:111
  136.6 4.6 %all-to-all-start.1 = ((bf16[8,2,16,512]{3,2,1,0:T(8,128)(2,1)}), bf16[8,2,16,512]{3,2,1,0:T(8,128)(2,1)S(1)}, u32[]{:S(2)}, u32[]{:S(2)}) async-start(bf16[8,2,16,512]{3,2,1,0:T(8,128)(2,1)} %copy.74), calls=%async_computation.2 | async-start | bytes 524288 | tf_op jit(solution)/shard_map/all_to_all | solution.py:114
  141.3 1.6 copy.75
  142.9 8.0 %all-to-all-done.1 = bf16[8,2,16,512]{3,2,1,0:T(8,128)(2,1)S(1)} async-done(((bf16[8,2,16,512]{3,2,1,0:T(8,128)(2,1)}), bf16[8,2,16,512]{3,2,1,0:T(8,128)(2,1)S(1)}, u32[]{:S(2)}, u32[]{:S(2)}) %all-to-all-start.1) | async-done | bytes 262176 | tf_op jit(solution)/shard_map/all_to_all | solution.py:114
  150.9 0.3 convolution_reduce_fusion
  151.3 0.7 add_convert_fusion
  (34 shorter events, 0.7 us)
Async XLA Ops:
  7.2 21.8 %copy-start = (bf16[256,2048]{1,0:T(8,128)(2,1)S(1)}, bf16[256,2048]{1,0:T(8,128)(2,1)}, u32[]{:S(2)}) copy-start(bf16[256,2048]{1,0:T(8,128)(2,1)} %param.26) | copy-start | bytes 3145732
  7.2 20.7 %copy-start.1 = (f32[2,16,16,64]{3,2,1,0:T(8,128)S(1)}, f32[2,16,16,64]{3,2,1,0:T(8,128)}, u32[]{:S(2)}) copy-start(f32[2,16,16,64]{3,2,1,0:T(8,128)} %param.24) | copy-start | bytes 393220
  7.2 21.8 %copy-start.5 = (f32[256]{0:T(256)S(1)}, f32[256]{0:T(256)}, u32[]{:S(2)}) copy-start(f32[256]{0:T(256)} %param.25) | copy-start | bytes 3076
  7.2 22.9 %copy-start.3 = (s32[64,2]{0,1:T(2,128)S(1)}, s32[64,2]{0,1:T(2,128)}, u32[]{:S(2)}) copy-start(s32[64,2]{0,1:T(2,128)} %param.32) | copy-start | bytes 1540
  7.2 60.4 %copy-start.2 = (f32[2048]{0:T(1024)S(1)}, f32[2048]{0:T(1024)}, u32[]{:S(2)}) copy-start(f32[2048]{0:T(1024)} %param.28) | copy-start | bytes 24580
  7.2 58.4 %all-gather.3.cloned.1.call-start = ((), (), s32[]{:S(2)}) async-start(), calls=%async_computation.4 | async-start | bytes 2621440 | tf_op jit(solution)/shard_map/all_gather | solution.py:97
  30.1 104.9 %reduce-scatter.2.cloned.1.call-start = ((), (), s32[]{:S(2)}) async-start(), calls=%async_computation.3 | async-start | bytes 1310720 | tf_op jit(solution)/shard_map/reduce_scatter | solution.py:111
  68.1 36.0 %slice-start.2 = ((s8[8388608]{0:T(1024)(128)(4,1)}), s8[4194304]{0:T(1024)(128)(4,1)S(1)}, s32[]{:S(2)}) async-start(s8[8388608]{0:T(1024)(128)(4,1)} %bitcast.114), calls=%async_computation.7 | async-start | bytes 8388608
  99.4 4.8 %slice-start.3 = ((s8[8388608]{0:T(1024)(128)(4,1)}), s8[4194304]{0:T(1024)(128)(4,1)S(1)}, s32[]{:S(2)}) async-start(s8[8388608]{0:T(1024)(128)(4,1)} %bitcast.114), calls=%async_computation.8 | async-start | bytes 8388608
  99.4 6.3 %slice-start = ((s8[8388608]{0:T(1024)(128)(4,1)}), s8[4194304]{0:T(1024)(128)(4,1)S(1)}, s32[]{:S(2)}) async-start(s8[8388608]{0:T(1024)(128)(4,1)} %bitcast.104), calls=%async_computation.5 | async-start | bytes 8388608
  104.2 2.5 %slice-start.1 = ((s8[8388608]{0:T(1024)(128)(4,1)}), s8[4194304]{0:T(1024)(128)(4,1)S(1)}, s32[]{:S(2)}) async-start(s8[8388608]{0:T(1024)(128)(4,1)} %bitcast.104), calls=%async_computation.6 | async-start | bytes 8388608
  106.6 44.3 %copy-start.4 = (f32[64,2]{0,1:T(2,128)S(1)}, f32[64,2]{0,1:T(2,128)}, u32[]{:S(2)}) copy-start(f32[64,2]{0,1:T(2,128)} %param.33) | copy-start | bytes 1540
  136.6 14.3 %all-to-all-start.1 = ((bf16[8,2,16,512]{3,2,1,0:T(8,128)(2,1)}), bf16[8,2,16,512]{3,2,1,0:T(8,128)(2,1)S(1)}, u32[]{:S(2)}, u32[]{:S(2)}) async-start(bf16[8,2,16,512]{3,2,1,0:T(8,128)(2,1)} %copy.74), calls=%async_computation.2 | async-start | bytes 524288 | tf_op jit(solution)/shard_map/all_to_all | solution.py:114
Sparse Core Ops, SparseCore 0:
  30.2 35.4 all-gather.2
  109.0 25.8 reduce-scatter.1
